TPU v7x, 256 devices: a whole 4x4x8 slice. The times are simulated.
256 devices in a mesh: sp: 32 (over z, y), tp: 8 (over x, core).
Axes of the slice: x: 4, y: 4, z: 8, core: 2. Of those that a mesh axis runs over, the one named last changes fastest.
Arguments:
- tokens: bfloat16 [4, 16384, 2048], P(None, ('sp', 'tp')), may hold values from -6 to 6
- in_gain: float32 [2048], replicated, may hold values from 0.1 to 1.9
- query_weight: bfloat16 [2048, 1024], P(None, 'tp'), may hold values from -0.125 to 0.125
- key_weight: bfloat16 [2048, 1024], P(None, 'tp'), may hold values from -0.125 to 0.125
- value_weight: bfloat16 [2048, 1024], P(None, 'tp'), may hold values from -0.125 to 0.125
- gate_weight: bfloat16 [2048, 1024], P(None, 'tp'), may hold values from -0.125 to 0.125
- log_decay: float32 [8], P('tp'), may hold values from -0.034 to 0, as said below
- norm_gain: float32 [1024], P('tp'), may hold values from 0.1 to 1.9
- out_weight: bfloat16 [1024, 2048], replicated, may hold values from -0.1875 to 0.1875
- post_gain: float32 [2048], replicated, may hold values from 0.1 to 1.9
Outputs:
- mixed: bfloat16 [4, 16384, 2048], P(None, ('sp', 'tp'))
Inputs may be any that keep to these rules, and one draw needn't show every extreme that they name: `log_decay`: every entry is negative; some heads keep a tenth or more of their memory over 16384 positions, others lose most of it within 30 to 100 positions.
All inputs are finite; a program needn't handle non-finite values.
Results may differ from a plain program's by a relative error of at most 0.015.
Values may be sent and summed in bfloat16 or wider, within the bound.
A program may use at most 64 MiB of HBM per device.

v0:
```python
import jax
import jax.numpy as jnp
from jax import lax
from jax.sharding import Mesh
from jax.sharding import PartitionSpec as P

HEAD_DIM = 128
BLOCK = 128
SP = ("sp_0", "sp_1")
SP_TP = ("sp_0", "sp_1", "tp")
rms_eps = 1e-06
group_eps = 1e-05
rope_base = 10000.0


def neutral_like(shard, identity):
    return jax.tree.map(
        lambda part, zero: jnp.zeros_like(part) + jnp.asarray(zero, part.dtype), shard, identity
    )


def entering(shard, axes, combine, identity):
    before = start = neutral_like(shard, identity)
    running = shard
    for axis in reversed(axes):
        length, mine = (lax.axis_size(axis), lax.axis_index(axis))
        pieces = jax.tree.map(lambda part: lax.all_gather(part, axis), running)
        inside, running = (start, start)
        for k in range(length):
            passed = k < mine
            running = combine(running, jax.tree.map(lambda part: part[k], pieces))
            inside = jax.tree.map(lambda new, old: jnp.where(passed, new, old), running, inside)
        before = combine(inside, before)
    return before


def rotate(values, positions):
    half_dim = values.shape[-1] // 2
    inverse = rope_base ** (-jnp.arange(half_dim, dtype=jnp.float32) / half_dim)
    angles = positions.astype(jnp.float32)[:, None] * inverse[None, :]
    cosine = jnp.cos(angles)
    sine_part = jnp.sin(angles)
    first_half = values[..., :half_dim].astype(jnp.float32)
    second = values[..., half_dim:].astype(jnp.float32)
    return jnp.concatenate(
        [first_half * cosine - second * sine_part, first_half * sine_part + second * cosine],
        axis=-1,
    )


def local_pass(queries, key_rows, values, log_decay):
    seq_count, head_count, length, head_width = queries.shape
    block_count = length // BLOCK
    offsets = jnp.arange(BLOCK, dtype=jnp.float32)
    distance = offsets[:, None] - offsets[None, :]
    rate_col = log_decay[:, None, None]
    inside = jnp.where(distance >= 0, jnp.exp(rate_col * jnp.maximum(distance, 0.0)), 0.0)
    query_scale = jnp.exp(log_decay[:, None] * (offsets + 1.0))[..., None]
    key_scale = jnp.exp(log_decay[:, None] * (BLOCK - 1.0 - offsets))[..., None]
    block_decay = jnp.exp(log_decay * BLOCK)[:, None, None]

    def to_blocks(arr):
        return arr.reshape(seq_count, head_count, block_count, BLOCK, arr.shape[-1]).transpose(
            2, 0, 1, 3, 4
        )

    def advance(memory, inputs):
        q_block, k_block, v_block = inputs
        scores = jnp.einsum("shqd,shkd->shqk", q_block, k_block, preferred_element_type=jnp.float32)
        weights = (scores * inside).astype(jnp.bfloat16)
        within = jnp.einsum("shqk,shkv->shqv", weights, v_block, preferred_element_type=jnp.float32)
        carried = jnp.einsum("shqd,shdv->shqv", q_block.astype(jnp.float32) * query_scale, memory)
        k_scaled = (k_block.astype(jnp.float32) * key_scale).astype(jnp.bfloat16)
        memory = memory * block_decay + jnp.einsum(
            "shkd,shkv->shdv", k_scaled, v_block, preferred_element_type=jnp.float32
        )
        return (memory, within + carried)

    start_memory = jnp.zeros((seq_count, head_count, head_width, values.shape[-1]), jnp.float32)
    end_state, outputs = lax.scan(
        advance, start_memory, (to_blocks(queries), to_blocks(key_rows), to_blocks(values))
    )
    outputs = outputs.transpose(1, 2, 0, 3, 4).reshape(
        seq_count, head_count, length, values.shape[-1]
    )
    return (outputs, end_state)


def combine(earlier, later_part):
    return (
        earlier[0] * later_part[0],
        earlier[1] * later_part[0][None, :, None, None] + later_part[1],
    )


def read_out(carried, queries, partial_out, log_decay):
    length = queries.shape[2]
    read_scale = jnp.exp(log_decay[:, None] * (jnp.arange(length, dtype=jnp.float32) + 1.0))[
        ..., None
    ]
    return partial_out + jnp.einsum(
        "shld,shdv->shlv", queries.astype(jnp.float32) * read_scale, carried
    )


def body(
    tokens,
    in_gain,
    query_weight,
    key_weight,
    value_weight,
    gate_weight,
    log_decay,
    norm_gain,
    out_weight,
    post_gain,
):
    seq_count, rows_dev, model_width = tokens.shape
    tp_size = lax.axis_size("tp")
    local_width = query_weight.shape[1]
    head_count = local_width // HEAD_DIM
    stretch = rows_dev * tp_size
    tok_f32 = tokens.astype(jnp.float32)
    normed = (
        tok_f32 * lax.rsqrt(jnp.mean(tok_f32 * tok_f32, axis=-1, keepdims=True) + rms_eps) * in_gain
    ).astype(jnp.bfloat16)
    joined = jnp.concatenate([query_weight, key_weight, value_weight, gate_weight], axis=1)
    projected = jnp.einsum(
        "kux,xt->kut",
        lax.all_gather(normed, "tp", axis=1, tiled=True),
        joined,
        preferred_element_type=jnp.float32,
    ).astype(jnp.bfloat16)

    def heads_of(columns):
        return columns.reshape(seq_count, stretch, head_count, HEAD_DIM).transpose(0, 2, 1, 3)

    positions = lax.axis_index(SP) * stretch + jnp.arange(stretch, dtype=jnp.int32)
    queries = rotate(heads_of(projected[..., :local_width]), positions).astype(jnp.bfloat16)
    key_rows = (
        rotate(heads_of(projected[..., local_width : 2 * local_width]), positions)
        * HEAD_DIM ** (-0.5)
    ).astype(jnp.bfloat16)
    values = heads_of(projected[..., 2 * local_width : 3 * local_width])
    gating = projected[..., 3 * local_width :]
    partial_out, end_state = local_pass(queries, key_rows, values, log_decay)
    span_decay = jnp.exp(log_decay * stretch)
    carried = entering(
        (span_decay, end_state), SP, combine, (jnp.ones_like(span_decay), jnp.zeros_like(end_state))
    )[1]
    retained = read_out(carried, queries, partial_out, log_decay)
    center = jnp.mean(retained, axis=-1, keepdims=True)
    spread = jnp.mean(jnp.square(retained - center), axis=-1, keepdims=True)
    normal = (
        ((retained - center) * lax.rsqrt(spread + group_eps))
        .transpose(0, 2, 1, 3)
        .reshape(seq_count, stretch, local_width)
    )
    gated = (normal * norm_gain * jax.nn.silu(gating.astype(jnp.float32))).astype(jnp.bfloat16)
    premix = jnp.einsum(
        "hor,rn->hon",
        lax.all_to_all(gated, "tp", split_axis=1, concat_axis=2, tiled=True),
        out_weight,
        preferred_element_type=jnp.float32,
    )
    mixed = (
        premix * lax.rsqrt(jnp.mean(premix * premix, axis=-1, keepdims=True) + rms_eps) * post_gain
    )
    return mixed.astype(jnp.bfloat16)


def solution(mesh):
    torus = Mesh(mesh.devices.reshape(8, 4, mesh.shape["tp"]), ("sp_0", "sp_1", "tp"))
    return jax.shard_map(
        body,
        mesh=torus,
        in_specs=(
            P(None, SP_TP, None),
            P(),
            P(None, "tp"),
            P(None, "tp"),
            P(None, "tp"),
            P(None, "tp"),
            P("tp"),
            P("tp"),
            P(),
            P(),
        ),
        out_specs=P(None, SP_TP, None),
        check_vma=False,
    )
```

profile of v0, /device:TPU:1, one launch (start us, length us, event | category | flops | bytes accessed | tf_op | source)
XLA Modules:
  0.0 204.7 jit_solution(9332395953188734523)
XLA Ops:
  6.5 1.6 fusion.44
  8.1 2.6 %fusion.46 = bf16[4,64,2048]{2,1,0:T(8,128)(2,1)} fusion(bf16[4,64,2048]{2,1,0:T(8,128)(2,1)} %param.12, f32[2048]{0:T(1024)} %param.13, f32[4,64]{1,0:T(4,128)S(1)} %add_rsqrt_fusion.2), kind=kLoop, calls=%fused_computation.48 | loop fusion | flops 2097152 | bytes 2106368 | tf_op jit(solution)/shard_map/convert_element_type | solution.py:126
  13.5 53.8 %all-gather.7.cloned.1.call-done = bf16[4,512,2048]{2,1,0:T(8,128)(2,1)} async-done(((bf16[4,64,2048]{2,1,0:T(8,128)(2,1)}), bf16[4,512,2048]{2,1,0:T(8,128)(2,1)}) %all-gather.7.cloned.1.call-update) | async-done | bytes 8388624 | tf_op jit(solution)/shard_map/all_gather | solution.py:130
  67.3 9.5 %fusion.54 = bf16[4,512,512]{1,2,0:T(8,128)(2,1)S(1)} fusion(bf16[4,512,2048]{2,1,0:T(8,128)(2,1)} %all-gather.7.cloned.1.call-done, bf16[2048,128]{0,1:T(8,128)(2,1)S(1)} %copy.42, bf16[2048,128]{0,1:T(8,128)(2,1)S(1)} %copy.41, bf16[2048,128]{0,1:T(8,128)(2,1)S(1)} %copy.40, bf16[2048,128]{0,1:T(8,128)(2,1)S(1)} %copy.39), kind=kOutput, calls=%fused_computation.59 | convolution fusion | flops 4304404480 | bytes 12582912 | tf_op jit(solution)/shard_map/kux,xt->kut/dot_general | solution.py:128
  76.9 1.0 slice_bitcast_fusion
  80.3 1.3 copy.44
  81.6 1.2 reshape_transpose_reshape.3
  84.8 11.9 %while.15 = (s32[]{:T(128)}, f32[4,1,128,128]{3,2,0,1:T(8,128)S(1)}, f32[4,4,1,128,128]{4,3,1,2,0:T(8,128)}, f32[1]{0:T(128)}, bf16[4,4,1,128,128]{4,3,1,2,0:T(8...) while((s32[]{:T(128)}, ...), condition=%wide.region_2.3_spmd.clone.clone.clone, body=%wide.region_1.2_spmd.clone.clone.clone.sunk | while | flops 67977728 | bytes 2496632 | solution.py:80
  86.5 0.9 fusion.147
  89.5 0.9 fusion.147
  92.5 0.9 fusion.147
  95.5 0.9 fusion.147
  98.8 8.4 %all-reduce = f32[4]{0:T(128)S(1)} all-reduce(f32[4]{0:T(128)S(1)} %exponential_dynamic-update-slice_fusion), channel_id=2, replica_groups=mesh['sp_0'=8,'sp_1'=4,'tp'=8] {'sp_1'}, use_global_device_ids=true, to_apply=%add | all-reduce | flops 4 | bytes 32
  107.9 1.3 slice_multiply_fusion
  109.9 12.2 %all-gather.11.cloned.1.call-done = f32[16,1,128,128]{3,2,1,0:T(8,128)} async-done(((f32[4,1,128,128]{3,2,1,0:T(8,128)}), f32[16,1,128,128]{3,2,1,0:T(8,128)}) %all-gather.11.cloned.1.call-update) | async-done | bytes 1048592 | tf_op jit(solution)/shard_map/all_gather | solution.py:27
  122.0 3.8 %slice_add_fusion.8 = f32[4,1,128,128]{3,2,1,0:T(8,128)} fusion(f32[16,1,128,128]{3,2,1,0:T(8,128)} %all-gather.11.cloned.1.call-done, f32[]{:T(128)} %bitcast.20, f32[]{:T(128)} %bitcast.18, f32[16,1,128,128]{3,2,0,1:T(8,128)} %bitcast.197, f32[]{:T(128)} %bitcast.16, f32[]{:T(128)} %bitcast.13), kind=kLoop, calls=%fused_computation.109 | loop fusion | flops 458752 | bytes 1310736 | tf_op jit(solution)/shard_map/add | solution.py:92
  126.4 1.3 dynamic-update-slice.1
  127.7 13.9 %all-reduce.1 = f32[8]{0:T(128)S(1)} all-reduce(f32[8]{0:T(128)S(1)} %dynamic-update-slice.1), channel_id=3, replica_groups=mesh['sp_0'=8,'sp_1'=4,'tp'=8] {'sp_0'}, use_global_device_ids=true, to_apply=%add.1 | all-reduce | flops 8 | bytes 64
  146.3 18.7 %all-gather.9.cloned.1.call-done = f32[8,4,1,128,128]{4,3,2,1,0:T(8,128)} async-done(((f32[1,4,1,128,128]{4,3,2,1,0:T(8,128)}), f32[8,4,1,128,128]{4,3,2,1,0:T(8,128)}) %all-gather.9.cloned.1.call-update) | async-done | bytes 2097168 | tf_op jit(solution)/shard_map/all_gather | solution.py:27
  165.1 7.9 %fusion.128 = (f32[4,512]{1,0:T(4,128)S(1)}, f32[4,512,128]{1,2,0:T(8,128)S(1)}) fusion(f32[4,512,128]{1,2,0:T(8,128)S(1)} %reshape.499, f32[8,4,1,128,128]{4,3,1,2,0:T(8,128)} %bitcast.204, f32[4,1,128,128]{3,2,1,0:T(8,128)S(1)} %copy-done.4, f32[16,1,128,128]{3,2,0,1:T(8,128)S(1)} %bitcast.198, f32[16,1,128,128]{3,2,1,0:T(8,128)S(1)} %copy-done.3, ...), kind=kOutput, calls=%fused_computation.175 | convolution fusion | flops 71170048 | bytes 5777468 | tf_op jit(solution)/shard_map/shld,shdv->shlv/dot_general | solution.py:101
  173.2 1.5 fusion.62
  175.0 18.3 %all_to_all.18 = bf16[4,512,128]{2,0,1:T(4,128)(2,1)S(1)} all-to-all(bf16[4,512,128]{2,0,1:T(4,128)(2,1)S(1)} %copy.65), channel_id=1, replica_groups=mesh['sp_0'=8,'sp_1'=4,'tp'=8] {'tp'}, dimensions={1} | all-to-all | bytes 1048576 | tf_op jit(solution)/shard_map/all_to_all | solution.py:162
  193.4 3.6 %multiply_reduce_fusion = (f32[4,64]{1,0:T(4,128)S(1)}, f32[4,64,2048]{2,1,0:T(8,128)S(1)}) fusion(bf16[1024,2048]{1,0:T(8,128)(2,1)} %param.20, bf16[4,8,8,8,128]{4,3,2,1,0:T(8,128)(2,1)S(1)} %bitcast.203), kind=kOutput, calls=%fused_computation.58 | convolution fusion | flops 1074790144 | bytes 6816768 | tf_op jit(solution)/shard_map/hor,rn->hon/dot_general | solution.py:160
  197.0 1.2 multiply_convert_fusion.2
  (91 shorter events, 19.6 us)
Async XLA Ops:
  6.5 4.3 %copy-start.8 = (bf16[2048,128]{1,0:T(8,128)(2,1)S(1)}, bf16[2048,128]{1,0:T(8,128)(2,1)}, u32[]{:S(2)}) copy-start(bf16[2048,128]{1,0:T(8,128)(2,1)} %param.14) | copy-start | bytes 1572868
  6.5 60.8 %all-gather.7.cloned.1.call-start = ((), (), s32[]{:S(2)}) async-start(), calls=%async_computation.1 | async-start | bytes 9437184 | tf_op jit(solution)/shard_map/all_gather | solution.py:130
  8.1 3.0 %copy-start.9 = (bf16[2048,128]{1,0:T(8,128)(2,1)S(1)}, bf16[2048,128]{1,0:T(8,128)(2,1)}, u32[]{:S(2)}) copy-start(bf16[2048,128]{1,0:T(8,128)(2,1)} %param.15) | copy-start | bytes 1572868
  10.8 1.0 copy-start.10
  10.8 1.3 copy-start.11
  10.8 111.2 %all-gather.11.cloned.1.call-start = ((), (), s32[]{:S(2)}) async-start(), calls=%async_computation.3 | async-start | bytes 1310720 | tf_op jit(solution)/shard_map/all_gather | solution.py:27
  76.9 1.5 copy-start.2
  78.3 0.7 copy-start.6
  78.4 0.8 copy-start.7
  83.2 1.2 copy-start.1
  84.8 12.8 %copy-start.15 = (u32[256]{0:T(256)S(1)}, u32[256]{0:T(256)}, u32[]{:S(2)}) copy-start(u32[256]{0:T(256)} %constant.86) | copy-start | bytes 3076
  84.8 41.1 %copy-start.14 = (u32[256]{0:T(256)S(1)}, u32[256]{0:T(256)}, u32[]{:S(2)}) copy-start(u32[256]{0:T(256)} %constant.91) | copy-start | bytes 3076
  96.7 0.7 copy-start
  96.7 48.7 %copy-start.5 = (f32[4,4,1,128,128]{4,3,1,2,0:T(8,128)S(1)}, f32[4,4,1,128,128]{4,3,1,2,0:T(8,128)}, u32[]{:S(2)}) copy-start(f32[4,4,1,128,128]{4,3,1,2,0:T(8,128)} %get-tuple-element.58) | copy-start | bytes 3145732
  97.5 67.6 %all-gather.9.cloned.1.call-start = ((), (), s32[]{:S(2)}) async-start(), calls=%async_computation.2 | async-start | bytes 2359296 | tf_op jit(solution)/shard_map/all_gather | solution.py:27
  145.5 19.6 %copy-start.3 = (f32[16,1,128,128]{3,2,1,0:T(8,128)S(1)}, f32[16,1,128,128]{3,2,1,0:T(8,128)}, u32[]{:S(2)}) copy-start(f32[16,1,128,128]{3,2,1,0:T(8,128)} %all-gather.11.cloned.1.call-done) | copy-start | bytes 3145732
  145.5 19.6 %copy-start.4 = (f32[4,1,128,128]{3,2,1,0:T(8,128)S(1)}, f32[4,1,128,128]{3,2,1,0:T(8,128)}, u32[]{:S(2)}) copy-start(f32[4,1,128,128]{3,2,1,0:T(8,128)} %slice_add_fusion.8) | copy-start | bytes 786436
  165.1 8.1 %copy-start.13 = (f32[128]{0:T(128)S(1)}, f32[128]{0:T(128)}, u32[]{:S(2)}) copy-start(f32[128]{0:T(128)} %param.19) | copy-start | bytes 1540
  193.4 3.6 %copy-start.12 = (f32[2048]{0:T(1024)S(1)}, f32[2048]{0:T(1024)}, u32[]{:S(2)}) copy-start(f32[2048]{0:T(1024)} %param.21) | copy-start | bytes 24580
Sparse Core Ops, SparseCore 0:
  10.9 56.3 all-gather.6
  97.6 24.3 all-gather.10
  126.0 39.0 all-gather.8
where the time goes:
time: 205 us
  waiting for transfers between devices  84.8 us (41%)
  blocking collectives  40.6 us (20%)
  matrix products  27.4 us (13%)
  other arithmetic  20.4 us (10%)
  between operations  18 us (9%)
  local copies, waits for them, and re-layouts  13.3 us (6%)
    all_gather x1, waiting for transfers between devices, body(): lax.all_gather(normed, 'tp', axis=1, tiled=True)  53.8 us
    all_gather x2, waiting for transfers between devices, entering(): pieces = jax.tree.map(lambda part: lax.all_gather(part, axis), running)  30.9 us
    unnamed x2, blocking collectives  22.3 us
    all_to_all x1, blocking collectives, body(): lax.all_to_all(gated, 'tp', split_axis=1, concat_axis=2, tiled=True)  18.3 us
    dot_general x1, matrix products, body(): jnp.einsum('kux,xt->kut', lax.all_gather(normed, 'tp', axis=1, tiled=True...  9.51 us
    dot_general x1, matrix products, read_out(): jnp.einsum('shld,shdv->shlv', queries.astype(jnp.float32) * read_scale, c...  7.93 us
    unnamed x41, local copies, waits for them, and re-layouts  6.03 us
  transfers between devices with their start and end apart: 3, of which 3 were waited for; matrix products, arithmetic and copies ran while one was open for 4% of the time, Pallas kernels for 0%

commit v1 on v0

--- a/solution.py
+++ b/solution.py
@@ -159,7 +159,10 @@
     gated = (normal * norm_gain * jax.nn.silu(gating.astype(jnp.float32))).astype(jnp.bfloat16)
     premix = jnp.einsum(
         "hor,rn->hon",
-        lax.all_to_all(gated, "tp", split_axis=1, concat_axis=2, tiled=True),
+        jnp.concatenate(
+            lax.all_to_all(jnp.stack(jnp.split(gated, lax.axis_size("tp"), axis=1)), "tp", 0, 0),
+            axis=2,
+        ),
         out_weight,
         preferred_element_type=jnp.float32,
     )

time: 205 us -> 197 us (0.961)
  local copies, waits for them, and re-layouts: 13.3 us -> 5.68 us
  matrix products: 27.4 us -> 24.5 us
    concatenate x8 -> x0, local copies, waits for them, and re-layouts: 2.8 us -> none  [rotate(): jnp.concatenate([first_half * cosine - second * sine_part, first_half * s...]
    unnamed x41 -> x40, local copies, waits for them, and re-layouts: 6.03 us -> 3.59 us
    dot_general x1, matrix products: 3.57 us -> 1.34 us  [body(): jnp.einsum('hor,rn->hon', jnp.concatenate(lax.all_to_all(jnp.stack(jnp.sp...]
where the time goes in v1:
time: 197 us
  waiting for transfers between devices  85.5 us (43%)
  blocking collectives  40.4 us (21%)
  matrix products  24.5 us (12%)
  other arithmetic  22.4 us (11%)
  between operations  18 us (9%)
  local copies, waits for them, and re-layouts  5.68 us (3%)
    all_gather x1, waiting for transfers between devices, body(): lax.all_gather(normed, 'tp', axis=1, tiled=True)  54.7 us
    all_gather x2, waiting for transfers between devices, entering(): pieces = jax.tree.map(lambda part: lax.all_gather(part, axis), running)  30.7 us
    unnamed x2, blocking collectives  22.1 us
    all_to_all x1, blocking collectives, body(): lax.all_to_all(jnp.stack(jnp.split(gated, lax.axis_size('tp'), axis=1)),...  18.3 us
    dot_general x1, matrix products, body(): jnp.einsum('kux,xt->kut', lax.all_gather(normed, 'tp', axis=1, tiled=True...  8.43 us
    dot_general x1, matrix products, read_out(): jnp.einsum('shld,shdv->shlv', queries.astype(jnp.float32) * read_scale, c...  8.33 us
  transfers between devices with their start and end apart: 3, of which 3 were waited for; matrix products, arithmetic and copies ran while one was open for 4% of the time, Pallas kernels for 0%

profile of v1, /device:TPU:1, one launch (start us, length us, event | category | flops | bytes accessed | tf_op | source)
XLA Modules:
  0.0 196.6 jit_solution(126385107892916549)
XLA Ops:
  6.5 1.5 fusion.44
  8.1 2.7 %fusion.46 = bf16[4,64,2048]{2,1,0:T(8,128)(2,1)} fusion(bf16[4,64,2048]{2,1,0:T(8,128)(2,1)} %param.12, f32[2048]{0:T(1024)} %param.13, f32[4,64]{1,0:T(4,128)S(1)} %add_rsqrt_fusion.2), kind=kLoop, calls=%fused_computation.48 | loop fusion | flops 2097152 | bytes 2106368 | tf_op jit(solution)/shard_map/convert_element_type | solution.py:126
  11.7 1.0 multiply_cosine_fusion
  12.6 54.7 %all-gather.7.cloned.1.call-done = bf16[4,512,2048]{2,1,0:T(8,128)(2,1)} async-done(((bf16[4,64,2048]{2,1,0:T(8,128)(2,1)}), bf16[4,512,2048]{2,1,0:T(8,128)(2,1)}) %all-gather.7.cloned.1.call-update) | async-done | bytes 8388624 | tf_op jit(solution)/shard_map/all_gather | solution.py:130
  67.4 8.4 %fusion.54 = bf16[4,512,512]{2,1,0:T(8,128)(2,1)S(1)} fusion(bf16[4,512,2048]{2,1,0:T(8,128)(2,1)} %all-gather.7.cloned.1.call-done, bf16[2048,128]{1,0:T(8,128)(2,1)S(1)} %copy-done.8, bf16[2048,128]{1,0:T(8,128)(2,1)S(1)} %copy-done.9, bf16[2048,128]{1,0:T(8,128)(2,1)S(1)} %copy-done.10, bf16[2048,128]{1,0:T(8,128)(2,1)S(1)} %copy-done.11), kind=kOutput, calls=%fused_computation.59 | convolution fusion | flops 4304404480 | bytes 12582912 | tf_op jit(solution)/shard_map/kux,xt->kut/dot_general | solution.py:128
  76.2 0.8 fusion.58
  77.9 11.9 %while.15 = (s32[]{:T(128)}, f32[4,1,128,128]{3,2,0,1:T(8,128)S(1)}, f32[4,4,1,128,128]{4,3,1,2,0:T(8,128)}, f32[1]{0:T(128)}, bf16[4,4,1,128,128]{4,3,1,2,0:T(8...) while((s32[]{:T(128)}, ...), condition=%wide.region_2.3_spmd.clone.clone.clone, body=%wide.region_1.2_spmd.clone.clone.clone.sunk | while | flops 67977728 | bytes 2496632 | solution.py:80
  79.6 0.9 fusion.156
  82.6 0.9 fusion.156
  85.6 0.9 fusion.156
  88.5 0.9 fusion.156
  92.0 8.4 %all-reduce = f32[4]{0:T(128)S(1)} all-reduce(f32[4]{0:T(128)S(1)} %exponential_dynamic-update-slice_fusion), channel_id=2, replica_groups=mesh['sp_0'=8,'sp_1'=4,'tp'=8] {'sp_1'}, use_global_device_ids=true, to_apply=%add | all-reduce | flops 4 | bytes 32
  101.1 1.3 slice_multiply_fusion
  103.0 12.1 %all-gather.11.cloned.1.call-done = f32[16,1,128,128]{3,2,1,0:T(8,128)} async-done(((f32[4,1,128,128]{3,2,1,0:T(8,128)}), f32[16,1,128,128]{3,2,1,0:T(8,128)}) %all-gather.11.cloned.1.call-update) | async-done | bytes 1048592 | tf_op jit(solution)/shard_map/all_gather | solution.py:27
  115.1 3.8 %slice_add_fusion.8 = f32[4,1,128,128]{3,2,1,0:T(8,128)} fusion(f32[16,1,128,128]{3,2,1,0:T(8,128)} %all-gather.11.cloned.1.call-done, f32[]{:T(128)} %bitcast.26, f32[]{:T(128)} %bitcast.24, f32[16,1,128,128]{3,2,0,1:T(8,128)} %bitcast.223, f32[]{:T(128)} %bitcast.22, f32[]{:T(128)} %bitcast.19), kind=kLoop, calls=%fused_computation.114 | loop fusion | flops 458752 | bytes 1310736 | tf_op jit(solution)/shard_map/add | solution.py:92
  119.5 1.4 dynamic-update-slice.1
  120.9 13.7 %all-reduce.1 = f32[8]{0:T(128)S(1)} all-reduce(f32[8]{0:T(128)S(1)} %dynamic-update-slice.1), channel_id=3, replica_groups=mesh['sp_0'=8,'sp_1'=4,'tp'=8] {'sp_0'}, use_global_device_ids=true, to_apply=%add.1 | all-reduce | flops 8 | bytes 64
  138.5 1.0 copy.30
  139.6 18.6 %all-gather.9.cloned.1.call-done = f32[8,4,1,128,128]{4,3,2,1,0:T(8,128)} async-done(((f32[1,4,1,128,128]{4,3,2,1,0:T(8,128)}), f32[8,4,1,128,128]{4,3,2,1,0:T(8,128)}) %all-gather.9.cloned.1.call-update) | async-done | bytes 2097168 | tf_op jit(solution)/shard_map/all_gather | solution.py:27
  158.2 8.3 %fusion.136 = (f32[4,512]{1,0:T(4,128)S(1)}, f32[4,512,128]{2,1,0:T(8,128)S(1)}) fusion(f32[4,512,128]{2,1,0:T(8,128)} %bitcast.227, f32[8,4,1,128,128]{4,3,1,2,0:T(8,128)} %bitcast.228, f32[4,1,128,128]{3,2,1,0:T(8,128)S(1)} %copy-done.3, f32[16,1,128,128]{3,2,0,1:T(8,128)S(1)} %bitcast.224, f32[16,1,128,128]{3,2,1,0:T(8,128)S(1)} %copy-done.2, ...), kind=kOutput, calls=%fused_computation.194 | convolution fusion | flops 71170048 | bytes 6301756 | tf_op jit(solution)/shard_map/shld,shdv->shlv/dot_general | solution.py:101
  167.2 1.9 fusion.68
  169.2 18.3 %all_to_all.5 = bf16[8,4,64,128]{3,2,1,0:T(8,128)(2,1)S(1)} all-to-all(bf16[8,4,64,128]{3,2,1,0:T(8,128)(2,1)S(1)} %fusion.124), channel_id=1, replica_groups=mesh['sp_0'=8,'sp_1'=4,'tp'=8] {'tp'}, dimensions={0} | all-to-all | bytes 1048576 | tf_op jit(solution)/shard_map/all_to_all | solution.py:163
  187.5 1.3 multiply_reduce_fusion
  188.9 1.2 multiply_convert_fusion.2
  (78 shorter events, 14.1 us)
Async XLA Ops:
  6.5 60.9 %all-gather.7.cloned.1.call-start = ((), (), s32[]{:S(2)}) async-start(), calls=%async_computation.1 | async-start | bytes 9437184 | tf_op jit(solution)/shard_map/all_gather | solution.py:130
  8.1 59.3 %copy-start.8 = (bf16[2048,128]{1,0:T(8,128)(2,1)S(1)}, bf16[2048,128]{1,0:T(8,128)(2,1)}, u32[]{:S(2)}) copy-start(bf16[2048,128]{1,0:T(8,128)(2,1)} %param.17) | copy-start | bytes 1572868
  8.1 59.3 %copy-start.9 = (bf16[2048,128]{1,0:T(8,128)(2,1)S(1)}, bf16[2048,128]{1,0:T(8,128)(2,1)}, u32[]{:S(2)}) copy-start(bf16[2048,128]{1,0:T(8,128)(2,1)} %param.16) | copy-start | bytes 1572868
  8.1 59.3 %copy-start.10 = (bf16[2048,128]{1,0:T(8,128)(2,1)S(1)}, bf16[2048,128]{1,0:T(8,128)(2,1)}, u32[]{:S(2)}) copy-start(bf16[2048,128]{1,0:T(8,128)(2,1)} %param.15) | copy-start | bytes 1572868
  8.1 59.3 %copy-start.11 = (bf16[2048,128]{1,0:T(8,128)(2,1)S(1)}, bf16[2048,128]{1,0:T(8,128)(2,1)}, u32[]{:S(2)}) copy-start(bf16[2048,128]{1,0:T(8,128)(2,1)} %param.14) | copy-start | bytes 1572868
  10.9 104.3 %all-gather.11.cloned.1.call-start = ((), (), s32[]{:S(2)}) async-start(), calls=%async_computation.3 | async-start | bytes 1310720 | tf_op jit(solution)/shard_map/all_gather | solution.py:27
  75.8 1.3 copy-start.1
  77.9 12.8 %copy-start.13 = (u32[256]{0:T(256)S(1)}, u32[256]{0:T(256)}, u32[]{:S(2)}) copy-start(u32[256]{0:T(256)} %constant.86) | copy-start | bytes 3076
  77.9 41.1 %copy-start.12 = (u32[256]{0:T(256)S(1)}, u32[256]{0:T(256)}, u32[]{:S(2)}) copy-start(u32[256]{0:T(256)} %constant.91) | copy-start | bytes 3076
  89.8 0.7 copy-start
  89.8 48.7 %copy-start.4 = (f32[4,4,1,128,128]{4,3,1,2,0:T(8,128)S(1)}, f32[4,4,1,128,128]{4,3,1,2,0:T(8,128)}, u32[]{:S(2)}) copy-start(f32[4,4,1,128,128]{4,3,1,2,0:T(8,128)} %get-tuple-element.58) | copy-start | bytes 3145732
  90.6 67.6 %all-gather.9.cloned.1.call-start = ((), (), s32[]{:S(2)}) async-start(), calls=%async_computation.2 | async-start | bytes 2359296 | tf_op jit(solution)/shard_map/all_gather | solution.py:27
  115.1 43.1 %copy-start.2 = (f32[16,1,128,128]{3,2,1,0:T(8,128)S(1)}, f32[16,1,128,128]{3,2,1,0:T(8,128)}, u32[]{:S(2)}) copy-start(f32[16,1,128,128]{3,2,1,0:T(8,128)} %all-gather.11.cloned.1.call-done) | copy-start | bytes 3145732
  118.9 39.3 %copy-start.3 = (f32[4,1,128,128]{3,2,1,0:T(8,128)S(1)}, f32[4,1,128,128]{3,2,1,0:T(8,128)}, u32[]{:S(2)}) copy-start(f32[4,1,128,128]{3,2,1,0:T(8,128)} %slice_add_fusion.8) | copy-start | bytes 786436
  158.2 9.0 %copy-start.6 = (f32[128]{0:T(128)S(1)}, f32[128]{0:T(128)}, u32[]{:S(2)}) copy-start(f32[128]{0:T(128)} %param.19) | copy-start | bytes 1540
  167.2 20.3 %copy-start.7 = (bf16[1024,2048]{1,0:T(8,128)(2,1)S(1)}, bf16[1024,2048]{1,0:T(8,128)(2,1)}, u32[]{:S(2)}) copy-start(bf16[1024,2048]{1,0:T(8,128)(2,1)} %param.20) | copy-start | bytes 12582916
  187.5 1.4 copy-start.5
Sparse Core Ops, SparseCore 0:
  11.0 56.3 all-gather.6
  90.7 24.3 all-gather.10
  119.1 39.0 all-gather.8
